TPU v7x, 32 devices: a whole 2x2x4 slice. The times are simulated.
32 devices in a mesh: sp: 8 (over z, y), tp: 4 (over x, core).
Axes of the slice: x: 2, y: 2, z: 4, core: 2. Of those that a mesh axis runs over, the one named last changes fastest.
Arguments:
- tokens: bfloat16 [6144, 4096], P('sp', 'tp'), may hold values from -6 to 6
- in_proj: bfloat16 [3, 4096, 1024], P(None, 'tp', 'sp'), may hold values from -0.09375 to 0.09375
- group_mix: bfloat16 [3, 4, 256, 256], replicated, may hold values from -0.375 to 0.375
- pool_gain: float32 [3, 1024], replicated, may hold values from 0.1 to 1.9
- out_proj: bfloat16 [3, 1024, 4096], P(None, 'sp', 'tp'), may hold values from -0.1875 to 0.1875
- norm_gain: float32 [3, 4096], P(None, 'tp'), may hold values from 0.25 to 3
- norm_bias: float32 [3, 4096], P(None, 'tp'), may hold values from -1.5 to 1.5
Outputs:
- stream_out: bfloat16 [6144, 4096], P('sp', 'tp')
All inputs are finite; a program needn't handle non-finite values.
Results may differ from a plain program's by a relative error of at most 0.017.
Values may be sent and summed in bfloat16 or wider, within the bound.
A program may use at most 128 MiB of HBM per device.

v0:
```python
import jax
import jax.numpy as jnp
from jax import lax
from jax.sharding import PartitionSpec as P

pool_windows = (2, 4, 8, 16)
norm_eps = 1e-05


def padded(array, sides, width):
    for axis, dim in sides:
        devices, length = (lax.axis_size(axis), array.shape[dim])
        up = [(i, (i + 1) % devices) for i in range(devices - 1)]
        down = [(j, i) for i, j in up]
        last = lax.slice_in_dim(array, length - width, length, axis=dim)
        leading = lax.slice_in_dim(array, 0, width, axis=dim)
        before = lax.ppermute(last, axis, up)
        after = lax.ppermute(leading, axis, down)
        array = jnp.concatenate([before, array, after], axis=dim)
    return array


def on_device(tokens, in_proj, group_mix, pool_gain, out_proj, norm_gain, norm_bias):
    rows_dev = tokens.shape[0]
    feat_dev = tokens.shape[1]
    layer_count = in_proj.shape[0]
    pool_width = in_proj.shape[2] * lax.axis_size("sp")
    chan_share = pool_width // lax.axis_size("tp")
    group_width = group_mix.shape[2]
    model_width = feat_dev * lax.axis_size("tp")
    residual_scale = (2.0 * layer_count) ** 0.25
    fringe_width = max(pool_windows) // 2
    seq_length = rows_dev * lax.axis_size("sp")
    positions = lax.axis_index("sp") * rows_dev + jnp.arange(rows_dev)
    chan_groups = (lax.axis_index("tp") * chan_share + jnp.arange(chan_share)) // group_width
    in_all, out_all = (
        lax.all_gather(in_proj, "sp", axis=2, tiled=True),
        lax.all_gather(out_proj, "sp", axis=1, tiled=True),
    )
    stream = tokens
    for layer_idx in range(layer_count):
        in_block = in_all[layer_idx]
        out_block = out_all[layer_idx]
        projected = lax.psum_scatter(
            lax.dot_general(
                in_block, stream, (((0,), (1,)), ((), ())), preferred_element_type=jnp.float32
            ).astype(jnp.bfloat16),
            "tp",
            scatter_dimension=0,
            tiled=True,
        )
        extended = padded(projected, (("sp", 1),), fringe_width)
        ext_float = extended.astype(jnp.float32)
        pooled = jnp.zeros((chan_share, rows_dev), jnp.float32)
        for group_idx in range(4):
            own_rows = (chan_groups == group_idx)[:, None]
            span_len = pool_windows[group_idx]
            before = span_len // 2
            after = span_len - before
            window_total = jnp.zeros((ext_float.shape[0], rows_dev), jnp.float32)
            for offset in range(-before, after):
                window_total = (
                    window_total
                    + ext_float[:, fringe_width + offset : fringe_width + offset + rows_dev]
                )
            low_edge = jnp.clip(positions - before, 0, seq_length)
            high_edge = jnp.clip(positions + after, 0, seq_length)
            pooled = jnp.where(
                own_rows, window_total / (high_edge - low_edge).astype(jnp.float32)[None, :], pooled
            )
        differ = (pooled - projected.astype(jnp.float32)).astype(jnp.bfloat16)
        all_differ = lax.all_gather(differ, "tp", axis=0, tiled=True)
        grouped = all_differ.reshape(4, group_width, rows_dev)
        mixed_all = jnp.einsum(
            "gcd,gct->gdt", group_mix[layer_idx], grouped, preferred_element_type=jnp.float32
        ).reshape(pool_width, rows_dev)
        mixed_all = (mixed_all * pool_gain[layer_idx][:, None]).astype(jnp.bfloat16)
        branch = lax.dot_general(
            mixed_all, out_block, (((0,), (0,)), ((), ())), preferred_element_type=jnp.float32
        )
        resid = residual_scale * stream.astype(jnp.float32) + branch
        row_sums, squares = lax.psum((jnp.sum(resid, axis=1), jnp.sum(resid * resid, axis=1)), "tp")
        row_mean = row_sums / model_width
        row_var = squares / model_width - row_mean * row_mean
        normed = (resid - row_mean[:, None]) * lax.rsqrt(row_var[:, None] + norm_eps)
        stream = (normed * norm_gain[layer_idx][None, :] + norm_bias[layer_idx][None, :]).astype(
            jnp.bfloat16
        )
    return stream


def solution(mesh):
    in_specs = (
        P("sp", "tp"),
        P(None, "tp", "sp"),
        P(),
        P(),
        P(None, "sp", "tp"),
        P(None, "tp"),
        P(None, "tp"),
    )
    out_specs = P("sp", "tp")
    return jax.shard_map(
        on_device, mesh=mesh, in_specs=in_specs, out_specs=out_specs, check_vma=False
    )
```

profile of v0, /device:TPU:0, one launch (start us, length us, event | category | flops | bytes accessed | tf_op | source)
XLA Modules:
  0.0 468.3 jit_solution(7111326799867742258)
XLA Ops:
  7.3 104.3 %all-gather.6.cloned.1.call-done = bf16[3,1024,1024]{2,1,0:T(8,128)(2,1)} async-done(((bf16[3,1024,128]{2,1,0:T(8,128)(2,1)}), bf16[3,1024,1024]{2,1,0:T(8,128)(2,1)}) %all-gather.6.cloned.1.call-update) | async-done | bytes 6291472 | tf_op jit(solution)/shard_map/all_gather | solution.py:37
  111.6 5.0 %fusion.6 = bf16[1024,768]{1,0:T(8,128)(2,1)} fusion(bf16[768,1024]{1,0:T(8,128)(2,1)} %param.7, bf16[3,1024,1024]{2,1,0:T(8,128)(2,1)} %all-gather.6.cloned.1.call-done), kind=kOutput, calls=%fused_computation.24 | convolution fusion | flops 1611399168 | bytes 5242880 | tf_op jit(solution)/shard_map/dot_general | solution.py:45
  116.8 26.3 %reduce-scatter.4.cloned.1.call-done = bf16[256,768]{1,0:T(8,128)(2,1)} async-done(((bf16[1024,768]{1,0:T(8,128)(2,1)}), bf16[256,768]{1,0:T(8,128)(2,1)}) %reduce-scatter.4.cloned.1.call-update) | async-done | bytes 393232 | tf_op jit(solution)/shard_map/reduce_scatter | solution.py:44
  144.0 3.4 collective-permute-start
  149.3 4.3 collective-permute-done.1
  154.8 5.1 %fusion.44 = bf16[256,768]{1,0:T(8,128)(2,1)} fusion(bf16[256,768]{1,0:T(8,128)(2,1)} %reduce-scatter.4.cloned.1.call-done, f32[256,784]{1,0:T(8,128)S(1)} %maximum_convert_fusion, f32[768]{0:T(1024)S(1)} %get-tuple-element.41, f32[768]{0:T(1024)S(1)} %get-tuple-element.42, f32[768]{0:T(1024)S(1)} %get-tuple-element.43, f32[768]{0:T(1024)S(1)} %get-tuple-element.44, ...), kind=kLoop, calls=%fused_computation.83 | loop fusion | flops 7274496 | bytes 13382656 | tf_op jit(solution)/shard_map/convert_element_type | solution.py:71
  160.7 19.0 %all-gather.8.cloned.1.call-done = bf16[1024,768]{1,0:T(8,128)(2,1)} async-done(((bf16[256,768]{1,0:T(8,128)(2,1)}), bf16[1024,768]{1,0:T(8,128)(2,1)}) %all-gather.8.cloned.1.call-update) | async-done | bytes 1572880 | tf_op jit(solution)/shard_map/all_gather | solution.py:72
  181.7 98.7 %all-gather.10.cloned.1.call-done = bf16[3,1024,1024]{2,1,0:T(8,128)(2,1)} async-done(((bf16[3,128,1024]{2,1,0:T(8,128)(2,1)}), bf16[3,1024,1024]{2,1,0:T(8,128)(2,1)}) %all-gather.10.cloned.1.call-update) | async-done | bytes 6291472 | tf_op jit(solution)/shard_map/all_gather | solution.py:38
  280.5 5.8 %fusion.55 = (f32[768]{0:T(1024)S(1)}, f32[768]{0:T(1024)S(1)}, f32[768,1024]{1,0:T(8,128)}) fusion(bf16[1024,768]{1,0:T(8,128)(2,1)S(1)} %bitcast.86, bf16[3,1024,1024]{2,1,0:T(8,128)(2,1)} %all-gather.10.cloned.1.call-done, bf16[768,1024]{1,0:T(8,128)(2,1)} %param.7), kind=kOutput, calls=%fused_computation.119 | convolution fusion | flops 1615329792 | bytes 8394752 | tf_op jit(solution)/shard_map/dot_general | solution.py:78
  286.2 5.7 %all-reduce.2 = (f32[768]{0:T(1024)S(1)}, f32[768]{0:T(1024)S(1)}) all-reduce(f32[768]{0:T(1024)S(1)} %get-tuple-element.10, f32[768]{0:T(1024)S(1)} %get-tuple-element.9), channel_id=1, replica_groups=mesh['sp'=8,'tp'=4] {'tp'}, use_global_device_ids=true, to_apply=%region_4.5 | all-reduce | flops 1536 | bytes 12288 | tf_op jit(solution)/shard_map/psum | solution.py:82
  292.0 5.9 %fusion.10 = bf16[1024,768]{1,0:T(8,128)(2,1)} fusion(bf16[3,1024,1024]{2,1,0:T(8,128)(2,1)} %all-gather.6.cloned.1.call-done, f32[768,1024]{1,0:T(8,128)} %get-tuple-element.38, f32[1024]{0:T(1024)S(1)} %bitcast.95, f32[1024]{0:T(1024)S(1)} %bitcast.93, f32[768]{0:T(1024)S(1)} %get-tuple-element.37, f32[768]{0:T(1024)S(1)} %get-tuple-element.36), kind=kOutput, calls=%fused_computation.28 | convolution fusion | flops 1615331328 | bytes 6830080 | tf_op jit(solution)/shard_map/dot_general | solution.py:45
  298.0 26.6 %reduce-scatter.6.cloned.1.call-done = bf16[256,768]{1,0:T(8,128)(2,1)} async-done(((bf16[1024,768]{1,0:T(8,128)(2,1)}), bf16[256,768]{1,0:T(8,128)(2,1)}) %reduce-scatter.6.cloned.1.call-update) | async-done | bytes 393232 | tf_op jit(solution)/shard_map/reduce_scatter | solution.py:44
  330.8 4.3 collective-permute-done.3
  336.3 5.0 %fusion.45 = bf16[256,768]{1,0:T(8,128)(2,1)} fusion(bf16[256,768]{1,0:T(8,128)(2,1)} %reduce-scatter.6.cloned.1.call-done, f32[256,784]{1,0:T(8,128)S(1)} %maximum_convert_fusion.1, f32[768]{0:T(1024)S(1)} %get-tuple-element.41, f32[768]{0:T(1024)S(1)} %get-tuple-element.42, f32[768]{0:T(1024)S(1)} %get-tuple-element.43, f32[768]{0:T(1024)S(1)} %get-tuple-element.44, ...), kind=kLoop, calls=%fused_computation.84 | loop fusion | flops 7274496 | bytes 13382656 | tf_op jit(solution)/shard_map/convert_element_type | solution.py:71
  341.5 19.5 %all-gather.12.cloned.1.call-done = bf16[1024,768]{1,0:T(8,128)(2,1)} async-done(((bf16[256,768]{1,0:T(8,128)(2,1)}), bf16[1024,768]{1,0:T(8,128)(2,1)}) %all-gather.12.cloned.1.call-update) | async-done | bytes 1572880 | tf_op jit(solution)/shard_map/all_gather | solution.py:72
  363.5 5.9 %fusion.54 = (f32[768]{0:T(1024)S(1)}, f32[768]{0:T(1024)S(1)}, f32[768,1024]{1,0:T(8,128)}) fusion(bf16[1024,768]{1,0:T(8,128)(2,1)S(1)} %bitcast.85, bf16[3,1024,1024]{2,1,0:T(8,128)(2,1)} %all-gather.10.cloned.1.call-done, f32[1024]{0:T(1024)S(1)} %bitcast.96, f32[1024]{0:T(1024)S(1)} %bitcast.94, f32[768]{0:T(1024)S(1)} %get-tuple-element.37, ...), kind=kOutput, calls=%fused_computation.118 | convolution fusion | flops 1619261952 | bytes 9981952 | tf_op jit(solution)/shard_map/dot_general | solution.py:78
  369.3 6.0 %all-reduce.1 = (f32[768]{0:T(1024)S(1)}, f32[768]{0:T(1024)S(1)}) all-reduce(f32[768]{0:T(1024)S(1)} %get-tuple-element.8, f32[768]{0:T(1024)S(1)} %get-tuple-element.7), channel_id=1, replica_groups=mesh['sp'=8,'tp'=4] {'tp'}, use_global_device_ids=true, to_apply=%region_9.10 | all-reduce | flops 1536 | bytes 12288 | tf_op jit(solution)/shard_map/psum | solution.py:82
  375.3 5.9 %fusion.9 = bf16[1024,768]{1,0:T(8,128)(2,1)} fusion(bf16[3,1024,1024]{2,1,0:T(8,128)(2,1)} %all-gather.6.cloned.1.call-done, f32[768,1024]{1,0:T(8,128)} %get-tuple-element.39, f32[1024]{0:T(1024)S(1)} %bitcast.91, f32[1024]{0:T(1024)S(1)} %bitcast.89, f32[768]{0:T(1024)S(1)} %get-tuple-element.35, f32[768]{0:T(1024)S(1)} %get-tuple-element.34), kind=kOutput, calls=%fused_computation.27 | convolution fusion | flops 1615331328 | bytes 6830080 | tf_op jit(solution)/shard_map/dot_general | solution.py:45
  381.3 29.2 %reduce-scatter.8.cloned.1.call-done = bf16[256,768]{1,0:T(8,128)(2,1)} async-done(((bf16[1024,768]{1,0:T(8,128)(2,1)}), bf16[256,768]{1,0:T(8,128)(2,1)}) %reduce-scatter.8.cloned.1.call-update) | async-done | bytes 393232 | tf_op jit(solution)/shard_map/reduce_scatter | solution.py:44
  416.7 4.3 collective-permute-done.5
  422.2 5.0 %fusion.46 = bf16[256,768]{1,0:T(8,128)(2,1)} fusion(bf16[256,768]{1,0:T(8,128)(2,1)} %reduce-scatter.8.cloned.1.call-done, f32[256,784]{1,0:T(8,128)S(1)} %maximum_convert_fusion.2, f32[768]{0:T(1024)S(1)} %get-tuple-element.41, f32[768]{0:T(1024)S(1)} %get-tuple-element.42, f32[768]{0:T(1024)S(1)} %get-tuple-element.43, f32[768]{0:T(1024)S(1)} %get-tuple-element.44, ...), kind=kLoop, calls=%fused_computation.85 | loop fusion | flops 7274496 | bytes 13382656 | tf_op jit(solution)/shard_map/convert_element_type | solution.py:71
  427.2 19.8 %all-gather.14.cloned.1.call-done = bf16[1024,768]{1,0:T(8,128)(2,1)} async-done(((bf16[256,768]{1,0:T(8,128)(2,1)}), bf16[1024,768]{1,0:T(8,128)(2,1)}) %all-gather.14.cloned.1.call-update) | async-done | bytes 1572880 | tf_op jit(solution)/shard_map/all_gather | solution.py:72
  449.4 4.4 fusion.53
  453.7 6.0 %all-reduce = (f32[768]{0:T(1024)S(1)}, f32[768]{0:T(1024)S(1)}) all-reduce(f32[768]{0:T(1024)S(1)} %get-tuple-element.6, f32[768]{0:T(1024)S(1)} %get-tuple-element.5), channel_id=1, replica_groups=mesh['sp'=8,'tp'=4] {'tp'}, use_global_device_ids=true, to_apply=%region_14.15 | all-reduce | flops 1536 | bytes 12288 | tf_op jit(solution)/shard_map/psum | solution.py:82
  (59 shorter events, 29.3 us)
Async XLA Ops:
  6.5 105.1 %all-gather.6.cloned.1.call-start = ((), (), s32[]{:S(2)}) async-start(), calls=%async_computation.3 | async-start | bytes 7077888 | tf_op jit(solution)/shard_map/all_gather | solution.py:37
  7.3 135.8 %reduce-scatter.4.cloned.1.call-start = ((), (), s32[]{:S(2)}) async-start(), calls=%async_computation.4 | async-start | bytes 1966080 | tf_op jit(solution)/shard_map/reduce_scatter | solution.py:44
  116.7 63.0 %all-gather.8.cloned.1.call-start = ((), (), s32[]{:S(2)}) async-start(), calls=%async_computation.5 | async-start | bytes 1966080 | tf_op jit(solution)/shard_map/all_gather | solution.py:72
  144.0 5.3 %collective-permute-start = (bf16[256,8]{1,0:T(8,128)(2,1)S(1)}, bf16[256,8]{1,0:T(8,128)(2,1)S(1)}, u32[]{:S(2)}, u32[]{:S(2)}) collective-permute-start(bf16[256,8]{1,0:T(8,128)(2,1)S(1)} %get-tuple-element.24), channel_id=1, source_target_pairs={{0,4},{4,8},{8,12},{12,16},{16,20},{20,24},{24,28},{1,5},{5,9},{9,... | collective-permute-start | bytes 12296 | tf_op jit(solution)/shard_map/ppermute | solution.py:17
  147.4 6.2 %collective-permute-start.1 = (bf16[256,8]{1,0:T(8,128)(2,1)S(1)}, bf16[256,8]{1,0:T(8,128)(2,1)S(1)}, u32[]{:S(2)}, u32[]{:S(2)}) collective-permute-start(bf16[256,8]{1,0:T(8,128)(2,1)S(1)} %get-tuple-element.25), channel_id=1, source_target_pairs={{4,0},{8,4},{12,8},{16,12},{20,16},{24,20},{28,24},{5,1},{9,5},{13... | collective-permute-start | bytes 12296 | tf_op jit(solution)/shard_map/ppermute | solution.py:18
  154.8 5.8 %copy-start.1 = (f32[3,1024]{1,0:T(4,128)S(1)}, f32[3,1024]{1,0:T(4,128)}, u32[]{:S(2)}) copy-start(f32[3,1024]{1,0:T(4,128)} %param.10) | copy-start | bytes 36868
  154.8 5.8 %copy-start.2 = (f32[3,1024]{1,0:T(4,128)S(1)}, f32[3,1024]{1,0:T(4,128)}, u32[]{:S(2)}) copy-start(f32[3,1024]{1,0:T(4,128)} %param.12) | copy-start | bytes 36868
  154.8 5.8 %copy-start.3 = (f32[3,1024]{1,0:T(4,128)S(1)}, f32[3,1024]{1,0:T(4,128)}, u32[]{:S(2)}) copy-start(f32[3,1024]{1,0:T(4,128)} %param.13) | copy-start | bytes 36868
  154.8 24.9 %copy-start = (bf16[3,4,256,256]{3,2,1,0:T(8,128)(2,1)S(1)}, bf16[3,4,256,256]{3,2,1,0:T(8,128)(2,1)}, u32[]{:S(2)}) copy-start(bf16[3,4,256,256]{3,2,1,0:T(8,128)(2,1)} %param.9) | copy-start | bytes 4718596
  159.9 120.5 %all-gather.10.cloned.1.call-start = ((), (), s32[]{:S(2)}) async-start(), calls=%async_computation.6 | async-start | bytes 7077888 | tf_op jit(solution)/shard_map/all_gather | solution.py:38
  160.5 164.1 %reduce-scatter.6.cloned.1.call-start = ((), (), s32[]{:S(2)}) async-start(), calls=%async_computation.7 | async-start | bytes 1966080 | tf_op jit(solution)/shard_map/reduce_scatter | solution.py:44
  297.9 63.2 %all-gather.12.cloned.1.call-start = ((), (), s32[]{:S(2)}) async-start(), calls=%async_computation.8 | async-start | bytes 1966080 | tf_op jit(solution)/shard_map/all_gather | solution.py:72
  325.6 5.3 %collective-permute-start.2 = (bf16[256,8]{1,0:T(8,128)(2,1)S(1)}, bf16[256,8]{1,0:T(8,128)(2,1)S(1)}, u32[]{:S(2)}, u32[]{:S(2)}) collective-permute-start(bf16[256,8]{1,0:T(8,128)(2,1)S(1)} %get-tuple-element.22), channel_id=1, source_target_pairs={{0,4},{4,8},{8,12},{12,16},{16,20},{20,24},{24,28},{1,5},{5,9},{9,... | collective-permute-start | bytes 12296 | tf_op jit(solution)/shard_map/ppermute | solution.py:17
  328.9 6.2 %collective-permute-start.3 = (bf16[256,8]{1,0:T(8,128)(2,1)S(1)}, bf16[256,8]{1,0:T(8,128)(2,1)S(1)}, u32[]{:S(2)}, u32[]{:S(2)}) collective-permute-start(bf16[256,8]{1,0:T(8,128)(2,1)S(1)} %get-tuple-element.23), channel_id=1, source_target_pairs={{4,0},{8,4},{12,8},{16,12},{20,16},{24,20},{28,24},{5,1},{9,5},{13... | collective-permute-start | bytes 12296 | tf_op jit(solution)/shard_map/ppermute | solution.py:18
  341.3 69.2 %reduce-scatter.8.cloned.1.call-start = ((), (), s32[]{:S(2)}) async-start(), calls=%async_computation.9 | async-start | bytes 1966080 | tf_op jit(solution)/shard_map/reduce_scatter | solution.py:44
  361.1 2.4 copy-start.4
  381.2 65.8 %all-gather.14.cloned.1.call-start = ((), (), s32[]{:S(2)}) async-start(), calls=%async_computation.10 | async-start | bytes 1966080 | tf_op jit(solution)/shard_map/all_gather | solution.py:72
  411.5 5.3 %collective-permute-start.4 = (bf16[256,8]{1,0:T(8,128)(2,1)S(1)}, bf16[256,8]{1,0:T(8,128)(2,1)S(1)}, u32[]{:S(2)}, u32[]{:S(2)}) collective-permute-start(bf16[256,8]{1,0:T(8,128)(2,1)S(1)} %get-tuple-element.20), channel_id=1, source_target_pairs={{0,4},{4,8},{8,12},{12,16},{16,20},{20,24},{24,28},{1,5},{5,9},{9,... | collective-permute-start | bytes 12296 | tf_op jit(solution)/shard_map/ppermute | solution.py:17
  414.8 6.2 %collective-permute-start.5 = (bf16[256,8]{1,0:T(8,128)(2,1)S(1)}, bf16[256,8]{1,0:T(8,128)(2,1)S(1)}, u32[]{:S(2)}, u32[]{:S(2)}) collective-permute-start(bf16[256,8]{1,0:T(8,128)(2,1)S(1)} %get-tuple-element.21), channel_id=1, source_target_pairs={{4,0},{8,4},{12,8},{16,12},{20,16},{24,20},{28,24},{5,1},{9,5},{13... | collective-permute-start | bytes 12296 | tf_op jit(solution)/shard_map/ppermute | solution.py:18
  447.0 2.4 copy-start.5
Sparse Core Ops, SparseCore 0:
  9.4 102.1 all-gather.5
  116.8 26.2 reduce-scatter.3
  160.1 19.5 all-gather.7
  181.7 98.6 all-gather.9
  298.0 26.4 reduce-scatter.5
  341.4 19.6 all-gather.11
  381.3 29.1 reduce-scatter.7
  427.3 19.6 all-gather.13
where the time goes:
time: 469 us; the launch traced here: 468 us
  waiting for transfers between devices  359 us (77%)
  matrix products  39.2 us (8%)
  other arithmetic  20.4 us (4%)
  blocking collectives  17.7 us (4%)
  starting transfers between devices  14.5 us (3%)
  between operations  13.8 us (3%)
    all_gather x1, waiting for transfers between devices, on_device(): lax.all_gather(in_proj, 'sp', axis=2, tiled=True)  104 us
    all_gather x1, waiting for transfers between devices, on_device(): lax.all_gather(out_proj, 'sp', axis=1, tiled=True)  98.7 us
    reduce_scatter x3, waiting for transfers between devices, on_device(): lax.psum_scatter(lax.dot_general(in_block, stream, (((0,), (1,)), ((), ()...  82.1 us
    all_gather x3, waiting for transfers between devices, on_device(): all_differ = lax.all_gather(differ, 'tp', axis=0, tiled=True)  58.3 us
    psum x3, blocking collectives, on_device(): lax.psum((jnp.sum(resid, axis=1), jnp.sum(resid * resid, axis=1)), 'tp')  17.7 us
    dot_general x3, matrix products, on_device(): lax.dot_general(in_block, stream, (((0,), (1,)), ((), ())), preferred_ele...  16.8 us
    dot_general x3, matrix products, on_device(): lax.dot_general(mixed_all, out_block, (((0,), (0,)), ((), ())), preferred...  16 us
    convert_element_type x3, other arithmetic, on_device(): differ = (pooled - projected.astype(jnp.float32)).astype(jnp.bfloat16)  15 us
  transfers between devices with their start and end apart: 14, of which 14 were waited for; matrix products, arithmetic and copies ran while one was open for 0% of the time, Pallas kernels for 0%

commit v1 on v0

--- a/solution.py
+++ b/solution.py
@@ -69,7 +69,14 @@
                 own_rows, window_total / (high_edge - low_edge).astype(jnp.float32)[None, :], pooled
             )
         differ = (pooled - projected.astype(jnp.float32)).astype(jnp.bfloat16)
-        all_differ = lax.all_gather(differ, "tp", axis=0, tiled=True)
+        ring = [differ]
+        for hop in range(3):
+            ring.append(lax.ppermute(ring[-1], "tp", [(dev, (dev + 1) % 4) for dev in range(4)]))
+        all_differ = jnp.roll(
+            jnp.concatenate(ring[::-1], axis=0),
+            (lax.axis_index("tp") + 1) * ring[0].shape[0],
+            axis=0,
+        )
         grouped = all_differ.reshape(4, group_width, rows_dev)
         mixed_all = jnp.einsum(
             "gcd,gct->gdt", group_mix[layer_idx], grouped, preferred_element_type=jnp.float32

time: 469 us -> 456 us (0.972)
  waiting for transfers between devices: 359 us -> 316 us
  other arithmetic: 20.4 us -> 49.9 us
    ppermute x0 -> x9, waiting for transfers between devices: none -> 64.6 us  [on_device(): lax.ppermute(ring[-1], 'tp', [(dev, (dev + 1) % 4) for dev in range(4)])]
    all_gather x3 -> x0, waiting for transfers between devices: 58.3 us -> none  [on_device(): all_differ = lax.all_gather(differ, 'tp', axis=0, tiled=True)]
    all_gather x1, waiting for transfers between devices: 98.7 us -> 51.5 us  [on_device(): lax.all_gather(out_proj, 'sp', axis=1, tiled=True)]
    concatenate x0 -> x3, other arithmetic: none -> 31.6 us  [on_device(): jnp.roll(jnp.concatenate(ring[::-1], axis=0), (lax.axis_index('tp') + 1)...]
  transfers between devices with their start and end apart: 14 -> 20, of which waited for: 14 -> 20; matrix products, arithmetic and copies ran while one was open for 0% -> 4% of each run, Pallas kernels for 0% -> 0%
where the time goes in v1:
time: 456 us; the launch traced here: 451 us
  waiting for transfers between devices  316 us (69%)
  other arithmetic  49.9 us (11%)
  matrix products  34.8 us (8%)
  blocking collectives  18.2 us (4%)
  starting transfers between devices  15 us (3%)
  between operations  13.7 us (3%)
    all_gather x1, waiting for transfers between devices, on_device(): lax.all_gather(in_proj, 'sp', axis=2, tiled=True)  104 us
    reduce_scatter x3, waiting for transfers between devices, on_device(): lax.psum_scatter(lax.dot_general(in_block, stream, (((0,), (1,)), ((), ()...  80.2 us
    ppermute x9, waiting for transfers between devices, on_device(): lax.ppermute(ring[-1], 'tp', [(dev, (dev + 1) % 4) for dev in range(4)])  64.6 us
    all_gather x1, waiting for transfers between devices, on_device(): lax.all_gather(out_proj, 'sp', axis=1, tiled=True)  51.5 us
    concatenate x3, other arithmetic, on_device(): jnp.roll(jnp.concatenate(ring[::-1], axis=0), (lax.axis_index('tp') + 1)...  31.6 us
    psum x3, blocking collectives, on_device(): lax.psum((jnp.sum(resid, axis=1), jnp.sum(resid * resid, axis=1)), 'tp')  18.2 us
    dot_general x3, matrix products, on_device(): lax.dot_general(in_block, stream, (((0,), (1,)), ((), ())), preferred_ele...  16.8 us
    dot_general x3, matrix products, on_device(): lax.dot_general(mixed_all, out_block, (((0,), (0,)), ((), ())), preferred...  16 us
  transfers between devices with their start and end apart: 20, of which 20 were waited for; matrix products, arithmetic and copies ran while one was open for 4% of the time, Pallas kernels for 0%

profile of v1, /device:TPU:0, one launch (start us, length us, event | category | flops | bytes accessed | tf_op | source)
XLA Modules:
  0.0 451.1 jit_solution(18260733876675316424)
XLA Ops:
  7.3 104.3 %all-gather.3.cloned.1.call-done = bf16[3,1024,1024]{2,1,0:T(8,128)(2,1)} async-done(((bf16[3,1024,128]{2,1,0:T(8,128)(2,1)}), bf16[3,1024,1024]{2,1,0:T(8,128)(2,1)}) %all-gather.3.cloned.1.call-update) | async-done | bytes 6291472 | tf_op jit(solution)/shard_map/all_gather | solution.py:37
  117.5 25.5 %reduce-scatter.4.cloned.1.call-done = bf16[256,768]{1,0:T(8,128)(2,1)} async-done(((bf16[1024,768]{1,0:T(8,128)(2,1)}), bf16[256,768]{1,0:T(8,128)(2,1)}) %reduce-scatter.4.cloned.1.call-update) | async-done | bytes 393232 | tf_op jit(solution)/shard_map/reduce_scatter | solution.py:44
  159.2 7.2 %collective-permute-done.2 = bf16[256,768]{1,0:T(8,128)(2,1)S(1)} collective-permute-done((bf16[256,768]{1,0:T(8,128)(2,1)S(1)}, bf16[256,768]{1,0:T(8,128)(2,1)S(1)}, u32[]{:S(2)}, u32[]{:S(2)}) %collective-permute-start.2) | collective-permute-done | bytes 393248 | tf_op jit(solution)/shard_map/ppermute | solution.py:74
  166.5 7.1 %collective-permute-done.3 = bf16[256,768]{1,0:T(8,128)(2,1)S(1)} collective-permute-done((bf16[256,768]{1,0:T(8,128)(2,1)S(1)}, bf16[256,768]{1,0:T(8,128)(2,1)S(1)}, u32[]{:S(2)}, u32[]{:S(2)}) %collective-permute-start.3) | collective-permute-done | bytes 393248 | tf_op jit(solution)/shard_map/ppermute | solution.py:74
  174.1 7.1 %collective-permute-done.4 = bf16[256,768]{1,0:T(8,128)(2,1)S(1)} collective-permute-done((bf16[256,768]{1,0:T(8,128)(2,1)S(1)}, bf16[256,768]{1,0:T(8,128)(2,1)S(1)}, u32[]{:S(2)}, u32[]{:S(2)}) %collective-permute-start.4) | collective-permute-done | bytes 393248 | tf_op jit(solution)/shard_map/ppermute | solution.py:74
  181.3 10.5 %fusion.26 = bf16[1024,768]{1,0:T(8,128)(2,1)S(1)} fusion(s32[]{:T(128)S(6)} %select_n.83, bf16[256,768]{1,0:T(8,128)(2,1)S(1)} %collective-permute-done.4, bf16[256,768]{1,0:T(8,128)(2,1)S(1)} %collective-permute-done.3, bf16[256,768]{1,0:T(8,128)(2,1)S(1)} %collective-permute-done.2, bf16[256,768]{1,0:T(8,128)(2,1)S(1)} %fusion.65), kind=kLoop, calls=%fused_computation.68 | loop fusion | flops 12582912 | bytes 3145732 | tf_op jit(solution)/shard_map/jit(_roll_dynamic)/concatenate | solution.py:75
  192.5 51.5 %all-gather.5.cloned.1.call-done = bf16[3,1024,1024]{2,1,0:T(8,128)(2,1)} async-done(((bf16[3,128,1024]{2,1,0:T(8,128)(2,1)}), bf16[3,1024,1024]{2,1,0:T(8,128)(2,1)}) %all-gather.5.cloned.1.call-update) | async-done | bytes 6291472 | tf_op jit(solution)/shard_map/all_gather | solution.py:38
  244.0 5.8 %fusion.76 = (f32[768]{0:T(1024)S(1)}, f32[768]{0:T(1024)S(1)}, f32[768,1024]{1,0:T(8,128)}) fusion(bf16[1024,768]{1,0:T(8,128)(2,1)S(1)} %bitcast.86, bf16[3,1024,1024]{2,1,0:T(8,128)(2,1)} %all-gather.5.cloned.1.call-done, bf16[768,1024]{1,0:T(8,128)(2,1)} %param.9), kind=kOutput, calls=%fused_computation.164 | convolution fusion | flops 1615329792 | bytes 8394752 | tf_op jit(solution)/shard_map/dot_general | solution.py:85
  249.8 5.7 %all-reduce.2 = (f32[768]{0:T(1024)S(1)}, f32[768]{0:T(1024)S(1)}) all-reduce(f32[768]{0:T(1024)S(1)} %get-tuple-element.11, f32[768]{0:T(1024)S(1)} %get-tuple-element.10), channel_id=1, replica_groups=mesh['sp'=8,'tp'=4] {'tp'}, use_global_device_ids=true, to_apply=%region_4.6 | all-reduce | flops 1536 | bytes 12288 | tf_op jit(solution)/shard_map/psum | solution.py:89
  255.5 5.9 %fusion.31 = bf16[1024,768]{1,0:T(8,128)(2,1)} fusion(bf16[3,1024,1024]{2,1,0:T(8,128)(2,1)} %all-gather.3.cloned.1.call-done, f32[768,1024]{1,0:T(8,128)} %get-tuple-element.39, f32[1024]{0:T(1024)S(1)} %bitcast.95, f32[1024]{0:T(1024)S(1)} %bitcast.93, f32[768]{0:T(1024)S(1)} %get-tuple-element.38, f32[768]{0:T(1024)S(1)} %get-tuple-element.37), kind=kOutput, calls=%fused_computation.73 | convolution fusion | flops 1615331328 | bytes 6830080 | tf_op jit(solution)/shard_map/dot_general | solution.py:45
  261.5 26.6 %reduce-scatter.6.cloned.1.call-done = bf16[256,768]{1,0:T(8,128)(2,1)} async-done(((bf16[1024,768]{1,0:T(8,128)(2,1)}), bf16[256,768]{1,0:T(8,128)(2,1)}) %reduce-scatter.6.cloned.1.call-update) | async-done | bytes 393232 | tf_op jit(solution)/shard_map/reduce_scatter | solution.py:44
  304.1 7.2 %collective-permute-done.7 = bf16[256,768]{1,0:T(8,128)(2,1)S(1)} collective-permute-done((bf16[256,768]{1,0:T(8,128)(2,1)S(1)}, bf16[256,768]{1,0:T(8,128)(2,1)S(1)}, u32[]{:S(2)}, u32[]{:S(2)}) %collective-permute-start.7) | collective-permute-done | bytes 393248 | tf_op jit(solution)/shard_map/ppermute | solution.py:74
  311.3 7.2 %collective-permute-done.8 = bf16[256,768]{1,0:T(8,128)(2,1)S(1)} collective-permute-done((bf16[256,768]{1,0:T(8,128)(2,1)S(1)}, bf16[256,768]{1,0:T(8,128)(2,1)S(1)}, u32[]{:S(2)}, u32[]{:S(2)}) %collective-permute-start.8) | collective-permute-done | bytes 393248 | tf_op jit(solution)/shard_map/ppermute | solution.py:74
  318.6 7.2 %collective-permute-done.9 = bf16[256,768]{1,0:T(8,128)(2,1)S(1)} collective-permute-done((bf16[256,768]{1,0:T(8,128)(2,1)S(1)}, bf16[256,768]{1,0:T(8,128)(2,1)S(1)}, u32[]{:S(2)}, u32[]{:S(2)}) %collective-permute-start.9) | collective-permute-done | bytes 393248 | tf_op jit(solution)/shard_map/ppermute | solution.py:74
  325.7 10.5 %fusion.19 = bf16[1024,768]{1,0:T(8,128)(2,1)S(1)} fusion(s32[]{:T(128)S(6)} %select_n.83, bf16[256,768]{1,0:T(8,128)(2,1)S(1)} %collective-permute-done.9, bf16[256,768]{1,0:T(8,128)(2,1)S(1)} %collective-permute-done.8, bf16[256,768]{1,0:T(8,128)(2,1)S(1)} %collective-permute-done.7, bf16[256,768]{1,0:T(8,128)(2,1)S(1)} %fusion.66), kind=kLoop, calls=%fused_computation.61 | loop fusion | flops 12582912 | bytes 3145732 | tf_op jit(solution)/shard_map/jit(_roll_dynamic)/concatenate | solution.py:75
  337.0 5.9 %fusion.75 = (f32[768]{0:T(1024)S(1)}, f32[768]{0:T(1024)S(1)}, f32[768,1024]{1,0:T(8,128)}) fusion(bf16[1024,768]{1,0:T(8,128)(2,1)S(1)} %bitcast.85, bf16[3,1024,1024]{2,1,0:T(8,128)(2,1)} %all-gather.5.cloned.1.call-done, f32[1024]{0:T(1024)S(1)} %bitcast.96, f32[1024]{0:T(1024)S(1)} %bitcast.94, f32[768]{0:T(1024)S(1)} %get-tuple-element.38, ...), kind=kOutput, calls=%fused_computation.163 | convolution fusion | flops 1619261952 | bytes 9981952 | tf_op jit(solution)/shard_map/dot_general | solution.py:85
  342.8 6.3 %all-reduce.1 = (f32[768]{0:T(1024)S(1)}, f32[768]{0:T(1024)S(1)}) all-reduce(f32[768]{0:T(1024)S(1)} %get-tuple-element.9, f32[768]{0:T(1024)S(1)} %get-tuple-element.8), channel_id=1, replica_groups=mesh['sp'=8,'tp'=4] {'tp'}, use_global_device_ids=true, to_apply=%region_9.11 | all-reduce | flops 1536 | bytes 12288 | tf_op jit(solution)/shard_map/psum | solution.py:89
  349.2 5.9 %fusion.30 = bf16[1024,768]{1,0:T(8,128)(2,1)} fusion(bf16[3,1024,1024]{2,1,0:T(8,128)(2,1)} %all-gather.3.cloned.1.call-done, f32[768,1024]{1,0:T(8,128)} %get-tuple-element.40, f32[1024]{0:T(1024)S(1)} %bitcast.91, f32[1024]{0:T(1024)S(1)} %bitcast.89, f32[768]{0:T(1024)S(1)} %get-tuple-element.36, f32[768]{0:T(1024)S(1)} %get-tuple-element.35), kind=kOutput, calls=%fused_computation.72 | convolution fusion | flops 1615331328 | bytes 6830080 | tf_op jit(solution)/shard_map/dot_general | solution.py:45
  355.1 28.1 %reduce-scatter.8.cloned.1.call-done = bf16[256,768]{1,0:T(8,128)(2,1)} async-done(((bf16[1024,768]{1,0:T(8,128)(2,1)}), bf16[256,768]{1,0:T(8,128)(2,1)}) %reduce-scatter.8.cloned.1.call-update) | async-done | bytes 393232 | tf_op jit(solution)/shard_map/reduce_scatter | solution.py:44
  399.3 7.2 %collective-permute-done.12 = bf16[256,768]{1,0:T(8,128)(2,1)S(1)} collective-permute-done((bf16[256,768]{1,0:T(8,128)(2,1)S(1)}, bf16[256,768]{1,0:T(8,128)(2,1)S(1)}, u32[]{:S(2)}, u32[]{:S(2)}) %collective-permute-start.12) | collective-permute-done | bytes 393248 | tf_op jit(solution)/shard_map/ppermute | solution.py:74
  406.5 7.2 %collective-permute-done.13 = bf16[256,768]{1,0:T(8,128)(2,1)S(1)} collective-permute-done((bf16[256,768]{1,0:T(8,128)(2,1)S(1)}, bf16[256,768]{1,0:T(8,128)(2,1)S(1)}, u32[]{:S(2)}, u32[]{:S(2)}) %collective-permute-start.13) | collective-permute-done | bytes 393248 | tf_op jit(solution)/shard_map/ppermute | solution.py:74
  413.7 7.2 %collective-permute-done.14 = bf16[256,768]{1,0:T(8,128)(2,1)S(1)} collective-permute-done((bf16[256,768]{1,0:T(8,128)(2,1)S(1)}, bf16[256,768]{1,0:T(8,128)(2,1)S(1)}, u32[]{:S(2)}, u32[]{:S(2)}) %collective-permute-start.14) | collective-permute-done | bytes 393248 | tf_op jit(solution)/shard_map/ppermute | solution.py:74
  420.9 10.5 %fusion.12 = bf16[1024,768]{1,0:T(8,128)(2,1)S(1)} fusion(s32[]{:T(128)S(6)} %select_n.83, bf16[256,768]{1,0:T(8,128)(2,1)S(1)} %collective-permute-done.14, bf16[256,768]{1,0:T(8,128)(2,1)S(1)} %collective-permute-done.13, bf16[256,768]{1,0:T(8,128)(2,1)S(1)} %collective-permute-done.12, bf16[256,768]{1,0:T(8,128)(2,1)S(1)} %fusion.67), kind=kLoop, calls=%fused_computation.54 | loop fusion | flops 12582912 | bytes 3145732 | tf_op jit(solution)/shard_map/jit(_roll_dynamic)/concatenate | solution.py:75
  436.5 6.1 %all-reduce = (f32[768]{0:T(1024)S(1)}, f32[768]{0:T(1024)S(1)}) all-reduce(f32[768]{0:T(1024)S(1)} %get-tuple-element.7, f32[768]{0:T(1024)S(1)} %get-tuple-element.6), channel_id=1, replica_groups=mesh['sp'=8,'tp'=4] {'tp'}, use_global_device_ids=true, to_apply=%region_14.16 | all-reduce | flops 1536 | bytes 12288 | tf_op jit(solution)/shard_map/psum | solution.py:89
  (71 shorter events, 63.5 us)
Async XLA Ops:
  6.5 105.1 %all-gather.3.cloned.1.call-start = ((), (), s32[]{:S(2)}) async-start(), calls=%async_computation.3 | async-start | bytes 7077888 | tf_op jit(solution)/shard_map/all_gather | solution.py:37
  7.3 135.8 %reduce-scatter.4.cloned.1.call-start = ((), (), s32[]{:S(2)}) async-start(), calls=%async_computation.4 | async-start | bytes 1966080 | tf_op jit(solution)/shard_map/reduce_scatter | solution.py:44
  116.7 127.3 %all-gather.5.cloned.1.call-start = ((), (), s32[]{:S(2)}) async-start(), calls=%async_computation.5 | async-start | bytes 7077888 | tf_op jit(solution)/shard_map/all_gather | solution.py:38
  117.4 170.6 %reduce-scatter.6.cloned.1.call-start = ((), (), s32[]{:S(2)}) async-start(), calls=%async_computation.6 | async-start | bytes 1966080 | tf_op jit(solution)/shard_map/reduce_scatter | solution.py:44
  144.0 5.3 %collective-permute-start = (bf16[256,8]{1,0:T(8,128)(2,1)S(1)}, bf16[256,8]{1,0:T(8,128)(2,1)S(1)}, u32[]{:S(2)}, u32[]{:S(2)}) collective-permute-start(bf16[256,8]{1,0:T(8,128)(2,1)S(1)} %get-tuple-element.25), channel_id=1, source_target_pairs={{0,4},{4,8},{8,12},{12,16},{16,20},{20,24},{24,28},{1,5},{5,9},{9,... | collective-permute-start | bytes 12296 | tf_op jit(solution)/shard_map/ppermute | solution.py:17
  147.4 6.2 %collective-permute-start.1 = (bf16[256,8]{1,0:T(8,128)(2,1)S(1)}, bf16[256,8]{1,0:T(8,128)(2,1)S(1)}, u32[]{:S(2)}, u32[]{:S(2)}) collective-permute-start(bf16[256,8]{1,0:T(8,128)(2,1)S(1)} %get-tuple-element.26), channel_id=1, source_target_pairs={{4,0},{8,4},{12,8},{16,12},{20,16},{24,20},{28,24},{5,1},{9,5},{13... | collective-permute-start | bytes 12296 | tf_op jit(solution)/shard_map/ppermute | solution.py:18
  154.8 19.3 %copy-start.2 = (f32[3,1024]{1,0:T(4,128)S(1)}, f32[3,1024]{1,0:T(4,128)}, u32[]{:S(2)}) copy-start(f32[3,1024]{1,0:T(4,128)} %param.14) | copy-start | bytes 36868
  154.8 19.3 %copy-start.3 = (f32[3,1024]{1,0:T(4,128)S(1)}, f32[3,1024]{1,0:T(4,128)}, u32[]{:S(2)}) copy-start(f32[3,1024]{1,0:T(4,128)} %param.15) | copy-start | bytes 36868
  159.1 32.7 %copy-start = (bf16[3,4,256,256]{3,2,1,0:T(8,128)(2,1)S(1)}, bf16[3,4,256,256]{3,2,1,0:T(8,128)(2,1)}, u32[]{:S(2)}) copy-start(bf16[3,4,256,256]{3,2,1,0:T(8,128)(2,1)} %param.11) | copy-start | bytes 4718596
  159.2 7.3 %collective-permute-start.2 = (bf16[256,768]{1,0:T(8,128)(2,1)S(1)}, bf16[256,768]{1,0:T(8,128)(2,1)S(1)}, u32[]{:S(2)}, u32[]{:S(2)}) collective-permute-start(bf16[256,768]{1,0:T(8,128)(2,1)S(1)} %fusion.65), channel_id=1, source_target_pairs={{0,1},{1,2},{2,3},{3,0},{4,5},{5,6},{6,7},{7,4},{8,9},{9,10},{10,1... | collective-permute-start | bytes 1179656 | tf_op jit(solution)/shard_map/ppermute | solution.py:74
  166.4 7.2 %collective-permute-start.3 = (bf16[256,768]{1,0:T(8,128)(2,1)S(1)}, bf16[256,768]{1,0:T(8,128)(2,1)S(1)}, u32[]{:S(2)}, u32[]{:S(2)}) collective-permute-start(bf16[256,768]{1,0:T(8,128)(2,1)S(1)} %collective-permute-done.2), channel_id=1, source_target_pairs={{0,1},{1,2},{2,3},{3,0},{4,5},{5,6},{6,7},{7,4},{8,9},{9,10},{10,1... | collective-permute-start | bytes 1179656 | tf_op jit(solution)/shard_map/ppermute | solution.py:74
  173.6 7.6 %collective-permute-start.4 = (bf16[256,768]{1,0:T(8,128)(2,1)S(1)}, bf16[256,768]{1,0:T(8,128)(2,1)S(1)}, u32[]{:S(2)}, u32[]{:S(2)}) collective-permute-start(bf16[256,768]{1,0:T(8,128)(2,1)S(1)} %collective-permute-done.3), channel_id=1, source_target_pairs={{0,1},{1,2},{2,3},{3,0},{4,5},{5,6},{6,7},{7,4},{8,9},{9,10},{10,1... | collective-permute-start | bytes 1179656 | tf_op jit(solution)/shard_map/ppermute | solution.py:74
  261.4 121.8 %reduce-scatter.8.cloned.1.call-start = ((), (), s32[]{:S(2)}) async-start(), calls=%async_computation.7 | async-start | bytes 1966080 | tf_op jit(solution)/shard_map/reduce_scatter | solution.py:44
  289.0 5.3 %collective-permute-start.5 = (bf16[256,8]{1,0:T(8,128)(2,1)S(1)}, bf16[256,8]{1,0:T(8,128)(2,1)S(1)}, u32[]{:S(2)}, u32[]{:S(2)}) collective-permute-start(bf16[256,8]{1,0:T(8,128)(2,1)S(1)} %get-tuple-element.23), channel_id=1, source_target_pairs={{0,4},{4,8},{8,12},{12,16},{16,20},{20,24},{24,28},{1,5},{5,9},{9,... | collective-permute-start | bytes 12296 | tf_op jit(solution)/shard_map/ppermute | solution.py:17
  292.4 6.2 %collective-permute-start.6 = (bf16[256,8]{1,0:T(8,128)(2,1)S(1)}, bf16[256,8]{1,0:T(8,128)(2,1)S(1)}, u32[]{:S(2)}, u32[]{:S(2)}) collective-permute-start(bf16[256,8]{1,0:T(8,128)(2,1)S(1)} %get-tuple-element.24), channel_id=1, source_target_pairs={{4,0},{8,4},{12,8},{16,12},{20,16},{24,20},{28,24},{5,1},{9,5},{13... | collective-permute-start | bytes 12296 | tf_op jit(solution)/shard_map/ppermute | solution.py:18
  304.1 7.3 %collective-permute-start.7 = (bf16[256,768]{1,0:T(8,128)(2,1)S(1)}, bf16[256,768]{1,0:T(8,128)(2,1)S(1)}, u32[]{:S(2)}, u32[]{:S(2)}) collective-permute-start(bf16[256,768]{1,0:T(8,128)(2,1)S(1)} %fusion.66), channel_id=1, source_target_pairs={{0,1},{1,2},{2,3},{3,0},{4,5},{5,6},{6,7},{7,4},{8,9},{9,10},{10,1... | collective-permute-start | bytes 1179656 | tf_op jit(solution)/shard_map/ppermute | solution.py:74
  311.3 7.2 %collective-permute-start.8 = (bf16[256,768]{1,0:T(8,128)(2,1)S(1)}, bf16[256,768]{1,0:T(8,128)(2,1)S(1)}, u32[]{:S(2)}, u32[]{:S(2)}) collective-permute-start(bf16[256,768]{1,0:T(8,128)(2,1)S(1)} %collective-permute-done.7), channel_id=1, source_target_pairs={{0,1},{1,2},{2,3},{3,0},{4,5},{5,6},{6,7},{7,4},{8,9},{9,10},{10,1... | collective-permute-start | bytes 1179656 | tf_op jit(solution)/shard_map/ppermute | solution.py:74
  318.5 7.2 %collective-permute-start.9 = (bf16[256,768]{1,0:T(8,128)(2,1)S(1)}, bf16[256,768]{1,0:T(8,128)(2,1)S(1)}, u32[]{:S(2)}, u32[]{:S(2)}) collective-permute-start(bf16[256,768]{1,0:T(8,128)(2,1)S(1)} %collective-permute-done.8), channel_id=1, source_target_pairs={{0,1},{1,2},{2,3},{3,0},{4,5},{5,6},{6,7},{7,4},{8,9},{9,10},{10,1... | collective-permute-start | bytes 1179656 | tf_op jit(solution)/shard_map/ppermute | solution.py:74
  318.5 18.4 %copy-start.4 = (f32[768,1024]{1,0:T(8,128)S(1)}, f32[768,1024]{1,0:T(8,128)}, u32[]{:S(2)}) copy-start(f32[768,1024]{1,0:T(8,128)} %get-tuple-element.39) | copy-start | bytes 9437188
  384.2 5.3 %collective-permute-start.10 = (bf16[256,8]{1,0:T(8,128)(2,1)S(1)}, bf16[256,8]{1,0:T(8,128)(2,1)S(1)}, u32[]{:S(2)}, u32[]{:S(2)}) collective-permute-start(bf16[256,8]{1,0:T(8,128)(2,1)S(1)} %get-tuple-element.21), channel_id=1, source_target_pairs={{0,4},{4,8},{8,12},{12,16},{16,20},{20,24},{24,28},{1,5},{5,9},{9,... | collective-permute-start | bytes 12296 | tf_op jit(solution)/shard_map/ppermute | solution.py:17
  387.6 6.2 %collective-permute-start.11 = (bf16[256,8]{1,0:T(8,128)(2,1)S(1)}, bf16[256,8]{1,0:T(8,128)(2,1)S(1)}, u32[]{:S(2)}, u32[]{:S(2)}) collective-permute-start(bf16[256,8]{1,0:T(8,128)(2,1)S(1)} %get-tuple-element.22), channel_id=1, source_target_pairs={{4,0},{8,4},{12,8},{16,12},{20,16},{24,20},{28,24},{5,1},{9,5},{13... | collective-permute-start | bytes 12296 | tf_op jit(solution)/shard_map/ppermute | solution.py:18
  399.3 7.3 %collective-permute-start.12 = (bf16[256,768]{1,0:T(8,128)(2,1)S(1)}, bf16[256,768]{1,0:T(8,128)(2,1)S(1)}, u32[]{:S(2)}, u32[]{:S(2)}) collective-permute-start(bf16[256,768]{1,0:T(8,128)(2,1)S(1)} %fusion.67), channel_id=1, source_target_pairs={{0,1},{1,2},{2,3},{3,0},{4,5},{5,6},{6,7},{7,4},{8,9},{9,10},{10,1... | collective-permute-start | bytes 1179656 | tf_op jit(solution)/shard_map/ppermute | solution.py:74
  406.5 7.2 %collective-permute-start.13 = (bf16[256,768]{1,0:T(8,128)(2,1)S(1)}, bf16[256,768]{1,0:T(8,128)(2,1)S(1)}, u32[]{:S(2)}, u32[]{:S(2)}) collective-permute-start(bf16[256,768]{1,0:T(8,128)(2,1)S(1)} %collective-permute-done.12), channel_id=1, source_target_pairs={{0,1},{1,2},{2,3},{3,0},{4,5},{5,6},{6,7},{7,4},{8,9},{9,10},{10,1... | collective-permute-start | bytes 1179656 | tf_op jit(solution)/shard_map/ppermute | solution.py:74
  413.7 7.2 %collective-permute-start.14 = (bf16[256,768]{1,0:T(8,128)(2,1)S(1)}, bf16[256,768]{1,0:T(8,128)(2,1)S(1)}, u32[]{:S(2)}, u32[]{:S(2)}) collective-permute-start(bf16[256,768]{1,0:T(8,128)(2,1)S(1)} %collective-permute-done.13), channel_id=1, source_target_pairs={{0,1},{1,2},{2,3},{3,0},{4,5},{5,6},{6,7},{7,4},{8,9},{9,10},{10,1... | collective-permute-start | bytes 1179656 | tf_op jit(solution)/shard_map/ppermute | solution.py:74
  (2 other events, 30.0 us)
Sparse Core Ops, SparseCore 0:
  9.4 102.1 all-gather.2
  116.8 26.2 reduce-scatter.3
  145.2 98.6 all-gather.4
  261.6 26.4 reduce-scatter.5
  355.2 27.9 reduce-scatter.7
